TPU v7x, 32 devices: a whole 2x2x4 slice. The times are simulated.
32 devices in a mesh: ep: 8 (over z, y), tp: 4 (over x, core).
Axes of the slice: x: 2, y: 2, z: 4, core: 2. Of those that a mesh axis runs over, the one named last changes fastest.
Arguments:
- first_input: bfloat16 [4096, 2048], P('ep'), may hold values from -120 to 120
- first_gain: bfloat16 [2048], replicated, may hold values from 0.099609375 to 1.8984375
- pool_inward: bfloat16 [2048, 1024], P(None, 'tp'), may hold values from -0.125 to 0.125
- pool_mixing: bfloat16 [4, 256, 256], P('tp'), may hold values from -0.375 to 0.375
- pool_scale: bfloat16 [1024], P('tp'), may hold values from 0.099609375 to 1.8984375
- pool_outward: bfloat16 [1024, 2048], P('tp'), may hold values from -0.1875 to 0.1875
- second_input: bfloat16 [2048, 2048], P('ep'), may hold values from -120 to 120
- second_gain: bfloat16 [2048], replicated, may hold values from 0.099609375 to 1.8984375
- route_ids: int32 [2048, 2], P('ep'), may hold values from 0 to 3, all different within a row; in each aligned block of 256 rows (0 to 255, 256 to 511, ...) at most 144 rows name the same one
- route_logits: float32 [2048, 2], P('ep'), may hold values from -6 to 6
- expert_gate: bfloat16 [8, 2048, 2048], P('ep', None, 'tp'), may hold values from -0.125 to 0.125
- expert_up: bfloat16 [8, 2048, 2048], P('ep', None, 'tp'), may hold values from -0.125 to 0.125
- expert_down: bfloat16 [8, 2048, 2048], P('ep', 'tp'), may hold values from -0.09375 to 0.09375
Outputs:
- first_out: bfloat16 [4096, 2048], P('ep', 'tp')
- second_out: bfloat16 [2048, 2048], P('ep', 'tp')
Inputs may be any that keep to these rules, and one draw needn't show every extreme that they name: `route_ids`: each row names two different experts. In each aligned block of 256 rows (the rows of one index of ep) no expert is named by more than 144 rows, and in some blocks one expert is named by exactly 144 rows.
All inputs are finite; a program needn't handle non-finite values.
Results may differ from a plain program's by a relative error of at most 0.012.
Values may be sent and summed in bfloat16 or wider, within the bound.
A program may use at most 64 MiB of HBM per device.

v0:
```python
import jax
import jax.numpy as jnp
from jax import lax
from jax.sharding import PartitionSpec as P

epsilon = 1e-06


def from_behind(value, axis, steps):
    count = lax.axis_size(axis)
    leading, last = (max(0, -steps), min(count, count - steps))
    return lax.ppermute(value, axis, [(source, source + steps) for source in range(leading, last)])


def rms_scaled(values, weights):
    widened = values.astype(jnp.float32)
    inverse = lax.rsqrt(jnp.mean(widened * widened, axis=-1, keepdims=True) + epsilon)
    return (widened * inverse * weights.astype(jnp.float32)).astype(jnp.bfloat16)


def window_means(channels, length, offset):
    row_count = channels.shape[0] - 15
    summed = jnp.zeros((row_count, channels.shape[1]), jnp.float32)
    for lookback in range(16):
        summed = summed + jnp.where(
            lookback < length, channels[15 - lookback : 15 - lookback + row_count], 0.0
        )
    positions = offset + jnp.arange(row_count, dtype=jnp.int32)
    counts = jnp.minimum(positions + 1, length).astype(jnp.float32)
    return summed / counts[:, None]


def slot_positions(block_ids, expert_count, capacity):
    flattened = block_ids.reshape(-1)
    onehot = (flattened[:, None] == jnp.arange(expert_count, dtype=jnp.int32)[None, :]).astype(
        jnp.int32
    )
    running = jnp.cumsum(onehot, axis=0, dtype=jnp.int32) - 1
    slot_numbers = jnp.sum(onehot * running, axis=1)
    return flattened * capacity + slot_numbers


def expert_output(gate_sum, up_sum, down_rows):
    hidden = (jax.nn.silu(gate_sum) * up_sum).astype(jnp.bfloat16)
    return jnp.dot(hidden, down_rows, preferred_element_type=jnp.float32)


def local(
    first_input,
    first_gain,
    pool_inward,
    pool_mixing,
    pool_scale,
    pool_outward,
    second_input,
    second_gain,
    route_ids,
    route_logits,
    expert_gate,
    expert_up,
    expert_down,
):
    tensor_parts = lax.axis_size("tp")
    expert_count = lax.axis_size("ep") // 2
    model_width = first_input.shape[1]
    quarter_width = model_width // tensor_parts
    normed_first = rms_scaled(first_input, first_gain)
    pooled_in = jnp.dot(normed_first, pool_inward, preferred_element_type=jnp.float32).astype(
        jnp.bfloat16
    )
    halo_rows = from_behind(pooled_in[-15:], "ep", 1)
    extended = jnp.concatenate([halo_rows, pooled_in], axis=0).astype(jnp.float32)
    window = jnp.left_shift(jnp.int32(2), lax.axis_index("tp"))
    sequence_start = lax.axis_index("ep") * first_input.shape[0]
    means = window_means(extended, window, sequence_start)
    mixed = (means - pooled_in.astype(jnp.float32)).astype(jnp.bfloat16)
    pooled = (
        jnp.dot(mixed, pool_mixing[0], preferred_element_type=jnp.float32)
        * pool_scale.astype(jnp.float32)
    ).astype(jnp.bfloat16)
    mixer_term = jnp.dot(pooled, pool_outward, preferred_element_type=jnp.float32)
    normed_second = rms_scaled(second_input, second_gain)
    row_count = second_input.shape[0]
    capacity = 2 * row_count * 9 // (8 * expert_count)
    positions = slot_positions(route_ids, expert_count, capacity)
    repeated = jnp.repeat(normed_second, 2, axis=0)
    repeated = lax.dynamic_slice_in_dim(
        repeated, lax.axis_index("tp") * quarter_width, quarter_width, 1
    )
    send_width = repeated.shape[1]
    buffer = (
        jnp.zeros((expert_count * capacity, send_width), jnp.bfloat16).at[positions].set(repeated)
    )
    paired = jnp.broadcast_to(
        buffer.reshape(expert_count, 1, capacity, send_width),
        (expert_count, 2, capacity, send_width),
    ).reshape(2 * expert_count, capacity, send_width)
    arrived = lax.all_to_all(paired, "ep", split_axis=0, concat_axis=0, tiled=True)
    flattened = arrived.reshape(-1, quarter_width)
    portion = lax.all_gather(flattened, "tp", axis=1, tiled=True)
    gate_rows = expert_gate[0]
    up_rows = expert_up[0]
    gate_sum = jnp.dot(portion, gate_rows, preferred_element_type=jnp.float32)
    up_sum = jnp.dot(portion, up_rows, preferred_element_type=jnp.float32)
    flat_term = expert_output(gate_sum, up_sum, expert_down[0])
    first_summed = lax.psum_scatter(
        mixer_term.astype(jnp.bfloat16), "tp", scatter_dimension=1, tiled=True
    )
    expert_summed = lax.psum_scatter(
        flat_term.astype(jnp.bfloat16), "tp", scatter_dimension=1, tiled=True
    )
    half_out = expert_summed.reshape(2 * expert_count, capacity, quarter_width)
    returned = lax.all_to_all(half_out, "ep", split_axis=0, concat_axis=0, tiled=True)
    route_out = jnp.sum(
        returned.reshape(expert_count, 2, capacity, quarter_width).astype(jnp.float32), axis=1
    ).reshape(-1, quarter_width)
    picked = route_out[positions].reshape(row_count, 2, quarter_width)
    shares = jax.nn.sigmoid(route_logits - route_logits[:, ::-1])
    second_out = jnp.sum(picked * shares[:, :, None], axis=1).astype(jnp.bfloat16)
    return (first_summed, second_out)


def solution(mesh):
    placed = (
        P("ep", None),
        P(),
        P(None, "tp"),
        P("tp", None, None),
        P("tp"),
        P("tp", None),
        P("ep", None),
        P(),
        P("ep", None),
        P("ep", None),
        P("ep", None, "tp"),
        P("ep", None, "tp"),
        P("ep", "tp", None),
    )
    return jax.shard_map(
        local, mesh=mesh, in_specs=placed, out_specs=(P("ep", "tp"), P("ep", "tp")), check_vma=False
    )
```

profile of v0, /device:TPU:0, one launch (start us, length us, event | category | flops | bytes accessed | tf_op | source)
XLA Modules:
  0.0 210.5 jit_solution(13853103682736092720)
XLA Ops:
  7.2 1.0 copy.17
  8.2 0.1 eq.29
  8.5 0.7 broadcast_multiply_fusion
  9.2 1.2 reduce-window.6
  10.4 0.2 slice_reduce_fusion
  10.6 0.2 reduce-window.9
  10.9 0.1 copy.16
  11.1 0.1 mul.96
  11.2 0.7 convert_element_type.79
  11.9 1.5 fusion.4
  13.4 0.3 fusion.6
  13.7 2.6 %broadcast_in_dim.44 = bf16[256,2,2048]{2,1,0:T(2,128)(2,1)} broadcast(bf16[256,2048]{1,0:T(8,128)(2,1)S(1)} %fusion.6), dimensions={0,2} | broadcast | bytes 3145728 | tf_op jit(solution)/shard_map/broadcast_in_dim | solution.py:86
  16.4 4.1 %reshape.103 = bf16[512,2048]{1,0:T(8,128)(2,1)} reshape(bf16[256,2,2048]{2,1,0:T(2,128)(2,1)} %broadcast_in_dim.44) | data formatting | bytes 4194304 | tf_op jit(solution)/shard_map/reshape | solution.py:86
  20.5 3.0 %scatter_custom_fusion = bf16[576,512]{1,0:T(8,128)(2,1)S(1)} fusion(s32[512]{0:T(512)S(1)} %bitcast.49, bf16[512,2048]{1,0:T(8,128)(2,1)} %reshape.103, s32[]{:T(128)} %constant.31.clone.1, s32[]{:T(128)S(6)} %select_n.145, bf16[]{:T(256)} %constant.27.clone.1), kind=kCustom, calls=%fused_computation.61 | custom fusion | bytes 1115140 | tf_op jit(solution)/shard_map/scatter | solution.py:92
  23.7 36.1 %all_to_all.10 = bf16[8,144,512]{2,1,0:T(8,128)(2,1)} all-to-all(bf16[8,144,512]{2,1,0:T(8,128)(2,1)S(1)} %bitcast.46), channel_id=1, replica_groups=mesh['ep'=8,'tp'=4] {'ep'}, dimensions={0} | all-to-all | bytes 2359296 | tf_op jit(solution)/shard_map/all_to_all | solution.py:98
  59.9 36.2 %all-gather.2.cloned.1.call-done = bf16[1152,2048]{1,0:T(8,128)(2,1)} async-done(((bf16[1152,512]{1,0:T(8,128)(2,1)}), bf16[1152,2048]{1,0:T(8,128)(2,1)}) %all-gather.2.cloned.1.call-update) | async-done | bytes 4718608 | tf_op jit(solution)/shard_map/all_gather | solution.py:100
  96.1 7.0 %fusion.11 = f32[1152,512]{1,0:T(8,128)} fusion(bf16[1152,2048]{1,0:T(8,128)(2,1)} %all-gather.2.cloned.1.call-done, bf16[1,2048,512]{2,1,0:T(8,128)(2,1)} %param.23), kind=kOutput, calls=%fused_computation.20 | convolution fusion | flops 2415919104 | bytes 9175040 | tf_op jit(solution)/shard_map/dot_general | solution.py:103
  103.1 11.0 %convolution_convert_fusion = bf16[1152,2048]{1,0:T(8,128)(2,1)} fusion(bf16[1,512,2048]{2,1,0:T(8,128)(2,1)S(1)} %copy-done, bf16[1152,2048]{1,0:T(8,128)(2,1)} %all-gather.2.cloned.1.call-done, f32[1152,512]{1,0:T(8,128)} %fusion.11, bf16[1,2048,512]{2,1,0:T(8,128)(2,1)} %param.24), kind=kOutput, calls=%fused_computation.2 | convolution fusion | flops 4837736448 | bytes 15990784 | tf_op jit(solution)/shard_map/dot_general | solution.py:45
  114.2 0.2 reduce-scatter.3.cloned.1.call-start
  114.4 0.4 copy-done.4
  114.8 2.2 %fusion = f32[512]{0:T(512)S(1)} fusion(bf16[512,2048]{1,0:T(8,128)(2,1)} %param.13), kind=kLoop, calls=%fused_computation.5 | loop fusion | flops 3145216 | bytes 2099200 | tf_op jit(solution)/shard_map/reduce_sum | solution.py:17
  117.1 2.0 fusion.15
  119.1 3.4 %collective-permute-start = (bf16[15,256]{1,0:T(8,128)(2,1)S(1)}, bf16[15,256]{1,0:T(8,128)(2,1)S(1)}, u32[]{:S(2)}, u32[]{:S(2)}) collective-permute-start(bf16[15,256]{1,0:T(8,128)(2,1)S(1)} %slice.78), channel_id=1, source_target_pairs={{0,4},{4,8},{8,12},{12,16},{16,20},{20,24},{24,28},{1,5},{5,9},{9,... | collective-permute-start | bytes 23048 | tf_op jit(solution)/shard_map/ppermute | solution.py:12
  122.7 1.3 collective-permute-done
  124.0 4.8 %convolution_convert_fusion.1 = bf16[512,2048]{1,0:T(8,128)(2,1)} fusion(bf16[256,2048]{1,0:T(8,128)(2,1)} %param.18, f32[256]{0:T(256)S(1)} %convert_element_type.74, bf16[512,256]{1,0:T(8,128)(2,1)S(1)} %fusion.15, f32[527,256]{1,0:T(8,128)S(1)} %maximum_convert_fusion, f32[512]{0:T(512)S(1)} %minimum_convert_fusion, pred[]{:T(512)S(6)} %gt.63, ...), kind=kOutput, calls=%fused_computation.9 | convolution fusion | flops 609878016 | bytes 11930640 | tf_op jit(solution)/shard_map/dot_general | solution.py:81
  128.8 33.3 %reduce-scatter.5.cloned.1.call-done = bf16[1152,512]{1,0:T(8,128)(2,1)} async-done(((bf16[1152,2048]{1,0:T(8,128)(2,1)}), bf16[1152,512]{1,0:T(8,128)(2,1)}) %reduce-scatter.5.cloned.1.call-update) | async-done | bytes 1179664 | tf_op jit(solution)/shard_map/reduce_scatter | solution.py:109
  162.1 5.5 %all-to-all-start.1 = ((bf16[8,144,512]{2,1,0:T(8,128)(2,1)}), bf16[8,144,512]{2,1,0:T(8,128)(2,1)}, u32[]{:S(2)}, u32[]{:S(2)}) async-start(bf16[8,144,512]{2,1,0:T(8,128)(2,1)} %bitcast.48), calls=%async_computation.3 | async-start | bytes 2359296 | tf_op jit(solution)/shard_map/all_to_all | solution.py:113
  167.9 28.3 %all-to-all-done.1 = bf16[8,144,512]{2,1,0:T(8,128)(2,1)} async-done(((bf16[8,144,512]{2,1,0:T(8,128)(2,1)}), bf16[8,144,512]{2,1,0:T(8,128)(2,1)}, u32[]{:S(2)}, u32[]{:S(2)}) %all-to-all-start.1) | async-done | bytes 1179680 | tf_op jit(solution)/shard_map/all_to_all | solution.py:113
  196.2 1.6 convert_reduce_fusion
  197.7 2.3 %gather_fusion = f32[512,512]{1,0:T(8,128)} fusion(f32[576,512]{1,0:T(8,128)S(1)} %bitcast.44, s32[1024]{0:T(1024)S(1)} %pad_clamp_fusion), kind=kCustom, calls=%fused_computation | custom fusion | bytes 2099200 | tf_op jit(solution)/shard_map/gather | solution.py:117
  200.1 1.8 reshape.108
  201.9 2.1 multiply_reduce_fusion
  (36 shorter events, 0.8 us)
Async XLA Ops:
  7.2 95.9 %copy-start = (bf16[1,512,2048]{2,1,0:T(8,128)(2,1)S(1)}, bf16[1,512,2048]{2,1,0:T(8,128)(2,1)}, u32[]{:S(2)}) copy-start(bf16[1,512,2048]{2,1,0:T(8,128)(2,1)} %param.25) | copy-start | bytes 6291460
  7.2 6.2 %copy-start.1 = (bf16[256,2048]{1,0:T(8,128)(2,1)S(1)}, bf16[256,2048]{1,0:T(8,128)(2,1)}, u32[]{:S(2)}) copy-start(bf16[256,2048]{1,0:T(8,128)(2,1)} %param.19) | copy-start | bytes 3145732
  7.2 88.9 %all-gather.2.cloned.1.call-start = ((), (), s32[]{:S(2)}) async-start(), calls=%async_computation.5 | async-start | bytes 5898240 | tf_op jit(solution)/shard_map/all_gather | solution.py:100
  59.8 102.3 %reduce-scatter.5.cloned.1.call-start = ((), (), s32[]{:S(2)}) async-start(), calls=%async_computation.6 | async-start | bytes 5898240 | tf_op jit(solution)/shard_map/reduce_scatter | solution.py:109
  114.1 0.7 copy-start.4
  114.2 89.8 %reduce-scatter.3.cloned.1.call-start = ((), (), s32[]{:S(2)}) async-start(), calls=%async_computation.4 | async-start | bytes 2621440 | tf_op jit(solution)/shard_map/reduce_scatter | solution.py:106
  114.8 2.2 %copy-start.2 = (bf16[512,2048]{1,0:T(8,128)(2,1)S(1)}, bf16[512,2048]{1,0:T(8,128)(2,1)}, u32[]{:S(2)}) copy-start(bf16[512,2048]{1,0:T(8,128)(2,1)} %param.13) | copy-start | bytes 6291460
  117.1 5.6 %copy-start.6 = (bf16[256]{0:T(256)(128)(2,1)S(1)}, bf16[256]{0:T(256)(128)(2,1)}, u32[]{:S(2)}) copy-start(bf16[256]{0:T(256)(128)(2,1)} %param.17) | copy-start | bytes 1540
  117.1 6.9 %copy-start.5 = (bf16[1,256,256]{2,1,0:T(8,128)(2,1)S(1)}, bf16[1,256,256]{2,1,0:T(8,128)(2,1)}, u32[]{:S(2)}) copy-start(bf16[1,256,256]{2,1,0:T(8,128)(2,1)} %param.16) | copy-start | bytes 393220
  119.1 4.8 %collective-permute-start = (bf16[15,256]{1,0:T(8,128)(2,1)S(1)}, bf16[15,256]{1,0:T(8,128)(2,1)S(1)}, u32[]{:S(2)}, u32[]{:S(2)}) collective-permute-start(bf16[15,256]{1,0:T(8,128)(2,1)S(1)} %slice.78), channel_id=1, source_target_pairs={{0,4},{4,8},{8,12},{12,16},{16,20},{20,24},{24,28},{1,5},{5,9},{9,... | collective-permute-start | bytes 23048 | tf_op jit(solution)/shard_map/ppermute | solution.py:12
  128.8 38.9 %copy-start.3 = (f32[256,2]{0,1:T(2,128)S(1)}, f32[256,2]{0,1:T(2,128)}, u32[]{:S(2)}) copy-start(f32[256,2]{0,1:T(2,128)} %param.22) | copy-start | bytes 6148
  162.1 34.0 %all-to-all-start.1 = ((bf16[8,144,512]{2,1,0:T(8,128)(2,1)}), bf16[8,144,512]{2,1,0:T(8,128)(2,1)}, u32[]{:S(2)}, u32[]{:S(2)}) async-start(bf16[8,144,512]{2,1,0:T(8,128)(2,1)} %bitcast.48), calls=%async_computation.3 | async-start | bytes 2359296 | tf_op jit(solution)/shard_map/all_to_all | solution.py:113
Sparse Core Ops, SparseCore 0:
  59.9 36.0 all-gather.1
  114.3 47.7 reduce-scatter.4
  165.2 31.1 reduce-scatter.2
where the time goes:
time: 211 us
  waiting for transfers between devices  99.1 us (47%)
  blocking collectives  36.1 us (17%)
  matrix products  24.9 us (12%)
  local copies, waits for them, and re-layouts  16.5 us (8%)
  between operations  14 us (7%)
  other arithmetic  10.7 us (5%)
  starting transfers between devices  9.25 us (4%)
    all_gather x1, waiting for transfers between devices, local(): portion = lax.all_gather(flattened, 'tp', axis=1, tiled=True)  36.2 us
    all_to_all x1, blocking collectives, local(): lax.all_to_all(paired, 'ep', split_axis=0, concat_axis=0, tiled=True)  36.1 us
    reduce_scatter x1, waiting for transfers between devices, local(): lax.psum_scatter(flat_term.astype(jnp.bfloat16), 'tp', scatter_dimension=...  33.3 us
    all_to_all x1, waiting for transfers between devices, local(): lax.all_to_all(half_out, 'ep', split_axis=0, concat_axis=0, tiled=True)  28.3 us
    dot_general x1, matrix products, expert_output(): return jnp.dot(hidden, down_rows, preferred_element_type=jnp.float32)  11 us
    dot_general x1, matrix products, local(): gate_sum = jnp.dot(portion, gate_rows, preferred_element_type=jnp.float32)  7.03 us
    all_to_all x1, starting transfers between devices, local(): lax.all_to_all(half_out, 'ep', split_axis=0, concat_axis=0, tiled=True)  5.52 us
    dot_general x1, matrix products, local(): jnp.dot(pooled, pool_outward, preferred_element_type=jnp.float32)  4.78 us
  transfers between devices with their start and end apart: 5, of which 4 were waited for; matrix products, arithmetic and copies ran while one was open for 8% of the time, Pallas kernels for 0%

commit v1 on v0

v1 whole, which is shorter than its diff:
```python
import functools

import jax
import jax.numpy as jnp
from jax import lax
from jax.experimental import pallas as pl
from jax.experimental.pallas import tpu as pltpu
from jax.sharding import PartitionSpec as P

EPS = 1e-06
MESH = pl.DeviceIdType.MESH
F32, BF16 = jnp.float32, jnp.bfloat16


def ring_order(n):
    order = [0]
    for step in range(1, n // 2 + 1):
        order.append(step)
        if n - step != step:
            order.append(n - step)
    return order


def rms(values, gain):
    wide = values.astype(F32)
    inverse = lax.rsqrt(jnp.mean(wide * wide, axis=-1, keepdims=True) + EPS)
    return (wide * inverse * gain).astype(BF16)


def body(
    n, parts, cap,
    first_hbm, gain1, inward_hbm, mixing, scale, outward_hbm, x2, gain2, ids, ids_t, logits,
    gate_hbm, up_hbm, down_hbm,
    out1, out2,
    first_v, inward_v, outward_v, gate_v, up_v, down_v, load_sem,
    normed, sent, portion, hidden, term, core_in, x_out, x_in, half_out, back, total,
    halo_out, halo_in, extended, mixed, pooled, mix_term, mix_core, mix_x_out, mix_x_in,
    z_send, z_recv, xs, xr, d1s, d1r, d2s, d2r,
    r1s, r1r, r2s, r2r, r3s, r3r, hs, hr, m1s, m1r, m2s, m2r,
):
    me = lax.axis_index("ep")
    t = lax.axis_index("tp")
    t_core = t + 1 - 2 * lax.rem(t, 2)
    t_x = lax.rem(t + 2, 4)
    t_diag = lax.rem(t_core + 2, 4)
    rows2, width = x2.shape
    w = width // parts
    order = ring_order(n)
    groups = 4
    per = n // groups
    group_rows = per * cap
    rows1 = first_v.shape[0]
    tile1 = 128

    def quarter(index):
        return pl.ds(pl.multiple_of(index * w, w), w)

    def spot(i):
        return pl.ds(i * cap, cap)

    def group(g):
        return pl.ds(g * group_rows, group_rows)

    loads = [
        pltpu.make_async_copy(src, dst, load_sem.at[k])
        for k, (src, dst) in enumerate((
            (first_hbm, first_v), (inward_hbm, inward_v), (outward_hbm, outward_v),
            (gate_hbm.at[0], gate_v), (up_hbm.at[0], up_v), (down_hbm.at[0], down_v)))
    ]
    for load in loads:
        load.start()

    barrier = pltpu.get_barrier_semaphore()
    for r in range(1, n):
        pl.semaphore_signal(barrier, inc=1, device_id=(lax.rem(me + r, n), t), device_id_type=MESH)
    for other in (t_core, t_x):
        pl.semaphore_signal(barrier, inc=1, device_id=(me, other), device_id_type=MESH)

    def remote(src, dst, ssem, rsem, ep, tp):
        return pltpu.make_async_remote_copy(
            src_ref=src, dst_ref=dst, send_sem=ssem, recv_sem=rsem,
            device_id=(ep, tp), device_id_type=MESH)

    def z_copy(i):
        return remote(sent.at[spot(i)], portion.at[spot(i), quarter(t)],
                      z_send.at[i], z_recv.at[i], lax.rem(me + order[i], n), t)

    def x_copy(i):
        piece = portion.at[spot(i), quarter(t)]
        return remote(piece, piece, xs.at[i], xr.at[i], me, t_x)

    def x_arrival(i):
        piece = portion.at[spot(i), quarter(t_x)]
        return remote(piece, piece, xs.at[i], xr.at[i], me, t_x)

    def d1_copy(i):
        piece = portion.at[spot(i), quarter(t)]
        return remote(piece, piece, d1s.at[i], d1r.at[i], me, t_core)

    def d1_arrival(i):
        piece = portion.at[spot(i), quarter(t_core)]
        return remote(piece, piece, d1s.at[i], d1r.at[i], me, t_core)

    def d2_copy(i):
        piece = portion.at[spot(i), quarter(t_x)]
        return remote(piece, piece, d2s.at[i], d2r.at[i], me, t_core)

    def d2_arrival(i):
        piece = portion.at[spot(i), quarter(t_diag)]
        return remote(piece, piece, d2s.at[i], d2r.at[i], me, t_core)

    def r1_copy(g, k):
        return remote(term.at[group(g), quarter((t_core, t_diag)[k])], core_in.at[k, group(g)],
                      r1s.at[g, k], r1r.at[g, k], me, t_core)

    def r2_copy(g):
        return remote(x_out.at[group(g)], x_in.at[group(g)], r2s.at[g], r2r.at[g], me, t_x)

    def r3_copy(i):
        return remote(half_out.at[spot(i)], back.at[spot(i)], r3s.at[i], r3r.at[i],
                      lax.rem(me + n - order[i], n), t)

    def m1_copy(k):
        return remote(mix_term.at[:, quarter((t_core, t_diag)[k])], mix_core.at[k],
                      m1s.at[k], m1r.at[k], me, t_core)

    def m2_copy():
        return remote(mix_x_out, mix_x_in, m2s, m2r, me, t_x)

    def halo_copy():
        return remote(halo_out, halo_in, hs, hr, lax.rem(me + 1, n), t)

    def norm_tile(j, carry):
        tile = pl.ds(pl.multiple_of(j * 64, 64), 64)
        normed[tile, :] = rms(x2[tile, :], gain2[...].astype(F32))
        return carry

    lax.fori_loop(0, rows2 // 64, norm_tile, None)

    before = (lax.broadcasted_iota(jnp.int32, (rows2, rows2), 0)
              < lax.broadcasted_iota(jnp.int32, (rows2, rows2), 1)).astype(BF16)
    places = lax.broadcasted_iota(jnp.int32, (cap, rows2), 0)

    def chosen(i):
        expert = lax.rem(me + order[i], n) // 2
        named = (ids_t[0:1, :] == expert) | (ids_t[1:2, :] == expert)
        flags = jnp.broadcast_to(jnp.where(named, 1.0, 0.0), (16, rows2)).astype(BF16)
        slots = jnp.dot(flags, before, preferred_element_type=F32)[0:1, :].astype(jnp.int32)
        slots = jnp.where(named, slots, -1)
        return jnp.where(places == slots, 1.0, 0.0).astype(BF16)

    pl.semaphore_wait(barrier, n + 1)
    for i in range(1, n):
        sent[spot(i), :] = jnp.dot(
            chosen(i), normed[:, quarter(t)], preferred_element_type=F32).astype(BF16)
        z_copy(i).start()
    own_rows = chosen(0)
    for q in range(parts):
        portion[spot(0), q * w:(q + 1) * w] = jnp.dot(
            own_rows, normed[:, q * w:(q + 1) * w], preferred_element_type=F32).astype(BF16)

    loads[0].wait()
    loads[1].wait()

    def inward_tile(j, carry):
        tile = pl.ds(pl.multiple_of(j * tile1, tile1), tile1)
        later = pl.ds(pl.multiple_of(j * tile1 + 16, 16), tile1)
        rows = rms(first_v[tile, :], gain1[...].astype(F32))
        product = jnp.dot(rows, inward_v[...], preferred_element_type=F32).astype(BF16)
        extended[later, :] = product.astype(F32)
        return carry

    lax.fori_loop(0, rows1 // tile1, inward_tile, None)
    halo_out[...] = extended[rows1:rows1 + 16, :].astype(BF16)
    halo_copy().start()

    def relay1(i):
        z_copy(i).wait_recv()
        x_copy(i).start()
        d1_copy(i).start()

    def relay2(i):
        x_arrival(i).wait_recv()
        d2_copy(i).start()

    def ready(i):
        d1_arrival(i).wait_recv()
        d2_arrival(i).wait_recv()

    def positions(g):
        return [i for i in range(g * per, (g + 1) * per) if i > 0]

    def relay(step, g):
        if g < groups:
            for i in positions(g):
                step(i)

    def compute(g):
        unit_tile = min(256, hidden.shape[1])

        def units(j, carry):
            cols = pl.ds(pl.multiple_of(j * unit_tile, unit_tile), unit_tile)
            gate = jnp.dot(portion[group(g), :], gate_v[:, cols], preferred_element_type=F32)
            up = jnp.dot(portion[group(g), :], up_v[:, cols], preferred_element_type=F32)
            hidden[:, cols] = (gate / (1.0 + jnp.exp(-gate)) * up).astype(BF16)
            return carry

        lax.fori_loop(0, hidden.shape[1] // unit_tile, units, None)

        def outs(j, carry):
            cols = quarter(j)
            term[group(g), cols] = jnp.dot(
                hidden[...], down_v[:, cols], preferred_element_type=F32).astype(BF16)
            return carry

        lax.fori_loop(0, parts, outs, None)
        for k in (1, 0):
            r1_copy(g, k).start()

    def over_x(g):
        r1_copy(g, 1).wait_recv()
        x_out[group(g), :] = (term[group(g), quarter(t_x)].astype(F32)
                              + core_in[1, group(g), :].astype(F32)).astype(BF16)
        r2_copy(g).start()

    def home(g):
        r1_copy(g, 0).wait_recv()
        r2_copy(g).wait_recv()
        half_out[group(g), :] = (term[group(g), quarter(t)].astype(F32)
                                 + core_in[0, group(g), :].astype(F32)
                                 + x_in[group(g), :].astype(F32)).astype(BF16)
        for i in positions(g):
            r3_copy(i).start()

    relay(relay1, 0)

    halo_copy().wait_recv()
    loads[2].wait()
    extended[0:16, :] = jnp.where(me == 0, 0.0, halo_in[...].astype(F32))
    lanes = min(128, extended.shape[1])
    counts = jnp.minimum(
        me * rows1 + 1 + lax.broadcasted_iota(jnp.int32, (rows1, lanes), 0),
        jnp.left_shift(jnp.int32(2), t)).astype(F32)
    for c in range(extended.shape[1] // lanes):
        cols = slice(c * lanes, (c + 1) * lanes)
        whole = extended[:, cols]
        running, picked = whole, whole
        for level in range(4):
            running = running + pltpu.roll(running, 1 << level, 0)
            picked = jnp.where(t >= level, running, picked)
        mixed[:, cols] = (picked[16:, :] / counts - whole[16:, :]).astype(BF16)
    pooled[...] = (jnp.dot(mixed[...], mixing[0], preferred_element_type=F32)
                   * scale[...].astype(F32)).astype(BF16)

    def outward_tile(j, carry):
        mix_term[:, quarter(j)] = jnp.dot(
            pooled[...], outward_v[:, quarter(j)], preferred_element_type=F32).astype(BF16)
        return carry

    lax.fori_loop(0, parts, outward_tile, None)
    m1_copy(1).start()
    m1_copy(0).start()

    relay(relay2, 0)
    relay(relay1, 1)
    m1_copy(1).wait_recv()
    mix_x_out[...] = (mix_term[:, quarter(t_x)].astype(F32)
                      + mix_core[1].astype(F32)).astype(BF16)
    m2_copy().start()
    for k in (3, 4, 5):
        loads[k].wait()
    relay(ready, 0)
    compute(0)
    relay(relay2, 1)
    relay(relay1, 2)
    over_x(0)
    relay(ready, 1)
    compute(1)
    relay(relay2, 2)
    relay(relay1, 3)
    over_x(1)
    home(0)
    relay(ready, 2)
    compute(2)
    relay(relay2, 3)
    over_x(2)
    home(1)
    relay(ready, 3)
    compute(3)
    over_x(3)
    home(2)

    m1_copy(0).wait_recv()
    m2_copy().wait_recv()
    out1[...] = (mix_term[:, quarter(t)].astype(F32) + mix_core[0].astype(F32)
                 + mix_x_in[...].astype(F32)).astype(BF16)

    after = (lax.broadcasted_iota(jnp.int32, (rows2, rows2), 1)
             < lax.broadcasted_iota(jnp.int32, (rows2, rows2), 0)).astype(BF16)
    tall = lax.broadcasted_iota(jnp.int32, (rows2, cap), 1)
    difference = logits[:, 0:1] - logits[:, 1:2]
    share0 = 1.0 / (1.0 + jnp.exp(-difference))
    share1 = 1.0 / (1.0 + jnp.exp(difference))

    def combine(i, source):
        expert = lax.rem(me + order[i], n) // 2
        is0, is1 = ids[:, 0:1] == expert, ids[:, 1:2] == expert
        named = is0 | is1
        flags = jnp.broadcast_to(jnp.where(named, 1.0, 0.0), (rows2, 128)).astype(BF16)
        slots = jnp.dot(after, flags, preferred_element_type=F32)[:, 0:1].astype(jnp.int32)
        slots = jnp.where(named, slots, -1)
        table = jnp.where(tall == slots, 1.0, 0.0).astype(BF16)
        share = jnp.where(is0, share0, jnp.where(is1, share1, 0.0))
        picked = share * jnp.dot(table, source[spot(i), :], preferred_element_type=F32)
        if i == 0:
            total[...] = picked
        else:
            total[...] += picked

    def gather(g):
        for i in positions(g):
            r3_copy(i).wait_recv()
            combine(i, back)

    combine(0, half_out)
    gather(0)
    gather(1)
    home(3)
    gather(2)
    gather(3)
    out2[...] = total[...].astype(BF16)

    for i in range(1, n):
        z_copy(i).wait_send()
        x_copy(i).wait_send()
        d1_copy(i).wait_send()
        d2_copy(i).wait_send()
        r3_copy(i).wait_send()
    for g in range(groups):
        r1_copy(g, 0).wait_send()
        r1_copy(g, 1).wait_send()
        r2_copy(g).wait_send()
    m1_copy(0).wait_send()
    m1_copy(1).wait_send()
    m2_copy().wait_send()
    halo_copy().wait_send()


def local(
    first_input, first_gain, pool_inward, pool_mixing, pool_scale, pool_outward,
    second_input, second_gain, route_ids, route_logits, expert_gate, expert_up, expert_down,
):
    n = lax.axis_size("ep")
    parts = lax.axis_size("tp")
    experts = n // 2
    rows1, width = first_input.shape
    rows2 = second_input.shape[0]
    w = width // parts
    cap = 2 * rows2 * 9 // (8 * experts)
    cap = -(-cap // 16) * 16
    channels = pool_inward.shape[1]
    units = expert_gate.shape[2]
    slots = n * cap
    dma = pltpu.SemaphoreType.DMA
    vmem = pl.BlockSpec(memory_space=pltpu.VMEM)
    anywhere = pl.BlockSpec(memory_space=pl.ANY)
    v = pltpu.VMEM
    scratch = [
        v((rows1, width), BF16), v((width, channels), BF16), v((channels, width), BF16),
        v((width, units), BF16), v((width, units), BF16), v((units, width), BF16), dma((6,)),
        v((rows2, width), BF16), v((slots, w), BF16), v((slots, width), BF16),
        v((slots // 4, units), BF16), v((slots, width), BF16), v((2, slots, w), BF16),
        v((slots, w), BF16), v((slots, w), BF16), v((slots, w), BF16), v((slots, w), BF16),
        v((rows2, w), F32),
        v((16, channels), BF16), v((16, channels), BF16), v((rows1 + 16, channels), F32),
        v((rows1, channels), BF16), v((rows1, channels), BF16), v((rows1, width), BF16),
        v((2, rows1, w), BF16), v((rows1, w), BF16), v((rows1, w), BF16),
        dma((n,)), dma((n,)), dma((n,)), dma((n,)), dma((n,)), dma((n,)), dma((n,)), dma((n,)),
        dma((4, 2)), dma((4, 2)), dma((4,)), dma((4,)), dma((n,)), dma((n,)),
        dma(()), dma(()), dma((2,)), dma((2,)), dma(()), dma(()),
    ]
    return pl.pallas_call(
        functools.partial(body, n, parts, cap),
        out_shape=(jax.ShapeDtypeStruct((rows1, w), BF16), jax.ShapeDtypeStruct((rows2, w), BF16)),
        in_specs=[anywhere, vmem, anywhere, vmem, vmem, anywhere, vmem, vmem, vmem, vmem, vmem,
                  anywhere, anywhere, anywhere],
        out_specs=(vmem, vmem),
        scratch_shapes=scratch,
        compiler_params=pltpu.CompilerParams(
            collective_id=0, has_side_effects=True, vmem_limit_bytes=60 * 1024 * 1024),
    )(
        first_input, first_gain[None, :], pool_inward, pool_mixing, pool_scale[None, :],
        pool_outward, second_input, second_gain[None, :], route_ids, route_ids.T, route_logits,
        expert_gate, expert_up, expert_down,
    )


def solution(mesh):
    placed = (
        P("ep", None), P(), P(None, "tp"), P("tp", None, None), P("tp"), P("tp", None),
        P("ep", None), P(), P("ep", None), P("ep", None),
        P("ep", None, "tp"), P("ep", None, "tp"), P("ep", "tp", None),
    )
    return jax.shard_map(
        local, mesh=mesh, in_specs=placed, out_specs=(P("ep", "tp"), P("ep", "tp")), check_vma=False
    )
```

time: 211 us -> 113 us (0.54)
  Pallas kernels: 0 us -> 101 us
  waiting for transfers between devices: 99.1 us -> 0 us
  blocking collectives: 36.1 us -> 0 us
  matrix products: 24.9 us -> 0 us
  between operations: 14 us -> 0.64 us
  other arithmetic: 10.7 us -> 0 us
  starting transfers between devices: 9.25 us -> 0 us
  local copies, waits for them, and re-layouts: 16.5 us -> 10.3 us
    pallas_call x0 -> x1, Pallas kernels: none -> 101 us  [local(): pl.pallas_call(functools.partial(body, n, parts, cap), out_shape=(jax.Sha...]
    all_gather x1 -> x0, waiting for transfers between devices: 36.2 us -> none  [local(): portion = lax.all_gather(flattened, 'tp', axis=1, tiled=True)]
    all_to_all x1 -> x0, blocking collectives: 36.1 us -> none  [local(): lax.all_to_all(paired, 'ep', split_axis=0, concat_axis=0, tiled=True)]
    reduce_scatter x2 -> x0, waiting for transfers between devices: 33.3 us -> none  [the longest x1 33.3 us: local(): lax.psum_scatter(flat_term.astype(jnp.bfloat16), 'tp', scatter_dimension=...]
    all_to_all x1 -> x0, waiting for transfers between devices: 28.3 us -> none  [local(): lax.all_to_all(half_out, 'ep', split_axis=0, concat_axis=0, tiled=True)]
    dot_general x4 -> x0, matrix products: 24.9 us -> none  [the longest x1 11 us: expert_output(): return jnp.dot(hidden, down_rows, preferred_element_type=jnp.float32)]
    reduce_sum x5 -> x0, other arithmetic: 7.39 us -> none  [the longest x2 3.73 us: rms_scaled(): jnp.mean(widened * widened, axis=-1, keepdims=True) + epsilon]
    reshape x2 -> x0, local copies, waits for them, and re-layouts: 5.96 us -> none  [the longest x1 4.12 us: local(): repeated = jnp.repeat(normed_second, 2, axis=0)]
  transfers between devices with their start and end apart: 5 -> 0, of which waited for: 4 -> 0; matrix products, arithmetic and copies ran while one was open for 8% -> 0% of each run, Pallas kernels for 0% -> 0%
where the time goes in v1:
time: 113 us; the launch traced here: 112 us
  Pallas kernels  101 us (89%)
  local copies, waits for them, and re-layouts  10.3 us (9%)
    pallas_call x1, Pallas kernels, local(): pl.pallas_call(functools.partial(body, n, parts, cap), out_shape=(jax.Sha...  101 us
    unnamed x4, local copies, waits for them, and re-layouts  6.49 us

profile of v1, /device:TPU:0, one launch (start us, length us, event | category | flops | bytes accessed | tf_op | source)
XLA Modules:
  0.0 112.1 jit_solution(11937541432082041751)
XLA Ops:
  0.6 1.2 %broadcast_in_dim.10.scale = bf16[1,256]{1,0:T(2,128)(2,1)} reshape(bf16[256]{0:T(256)(128)(2,1)} %param.17) | data formatting | bytes 1024 | tf_op jit(solution)/shard_map/broadcast_in_dim | solution.py:392
  1.9 1.3 %broadcast_in_dim.9.gain1 = bf16[1,2048]{1,0:T(2,128)(2,1)} reshape(bf16[2048]{0:T(1024)(128)(2,1)} %param.14) | data formatting | bytes 8192 | tf_op jit(solution)/shard_map/broadcast_in_dim | solution.py:392
  3.1 1.3 %broadcast_in_dim.11.gain2 = bf16[1,2048]{1,0:T(2,128)(2,1)} reshape(bf16[2048]{0:T(1024)(128)(2,1)} %param.20) | data formatting | bytes 8192 | tf_op jit(solution)/shard_map/broadcast_in_dim | solution.py:393
  4.4 1.5 %copy.16.logits = f32[256,2]{1,0:T(8,128)} copy(f32[256,2]{0,1:T(2,128)} %param.22) | data formatting | bytes 4096 | tf_op args[9]
  5.9 1.5 %copy.15.ids = s32[256,2]{1,0:T(8,128)} copy(s32[256,2]{0,1:T(2,128)} %param.21) | data formatting | bytes 4096 | tf_op args[8]
  7.4 101.2 %shard_map.140 = (bf16[512,512]{1,0:T(8,128)(2,1)}, bf16[256,512]{1,0:T(8,128)(2,1)}) custom-call(bf16[512,2048]{1,0:T(8,128)(2,1)} %first_hbm.1, bf16[1,2048]{1,0:T(2,128)(2,1)} %broadcast_in_dim.9.gain1, bf16[2048,256]{1,0:T(8,128)(2,1)} %inward_hbm.1, bf16[1,256,256]{2,1,0:T(8,128)(2,1)} %mixing.1, bf16[1,256]{1,0:T(2,128)(2,1)} %broadcast_in_dim.10.scale, ...), custom_call_target="tpu_custom_call" | custom-call | tf_op jit(solution)/shard_map/pallas_call | solution.py:382
  108.6 1.9 %copy.19 = bf16[512,512]{1,0:T(8,128)(2,1)} copy(bf16[512,512]{1,0:T(8,128)(2,1)} %get-tuple-element.4) | data formatting | bytes 1048576
  110.5 1.7 %copy.20 = bf16[256,512]{1,0:T(8,128)(2,1)} copy(bf16[256,512]{1,0:T(8,128)(2,1)} %get-tuple-element.5) | data formatting | bytes 524288

commit v2 on v1

v2 whole, which is shorter than its diff:
```python
import functools

import jax
import jax.numpy as jnp
from jax import lax
from jax.experimental import pallas as pl
from jax.experimental.pallas import tpu as pltpu
from jax.sharding import PartitionSpec as P

EPS = 1e-06
MESH = pl.DeviceIdType.MESH
F32, BF16 = jnp.float32, jnp.bfloat16


def ring_order(m):
    return [0] + sorted(range(1, m), key=lambda r: (-min(r, m - r), r))


def rms(values, gain):
    wide = values.astype(F32)
    inverse = lax.rsqrt(jnp.mean(wide * wide, axis=-1, keepdims=True) + EPS)
    return (wide * inverse * gain).astype(BF16)


def body(
    n, parts, cap,
    first_hbm, gains, inward_hbm, mixing, outward_hbm, x2, ids_t, logits_t,
    gate_hbm, up_hbm, down_hbm,
    out1, out2,
    first_v, inward_v, outward_v, gate_v, up_v, down_v, load_sem,
    normed, sent, portion, hidden, term, core_in, x_out, x_in, half_out, y_in, whole_out, back, total,
    halo_out, halo_in, extended, mixed, pooled, mix_term, mix_core, mix_x_out, mix_x_in,
    zs, zr, xs, xr, ds, dr, ys, yr,
    r1s, r1r, r2s, r2r, r3s, r3r, r4s, r4r, hs, hr, m1s, m1r, m2s, m2r,
):
    me = lax.axis_index("ep")
    t = lax.axis_index("tp")
    t_core = t + 1 - 2 * lax.rem(t, 2)
    t_x = lax.rem(t + 2, 4)
    t_diag = lax.rem(t_core + 2, 4)
    rows2, width = x2.shape
    w = width // parts
    m = n // 2
    a, b = me // 2, lax.rem(me, 2)
    me_y = 2 * a + 1 - b
    order = ring_order(m)
    groups = 4
    per = m // groups
    group_rows = 2 * per * cap
    rows1 = first_v.shape[0]
    tile1 = 128

    def quarter(index):
        return pl.ds(pl.multiple_of(index * w, w), w)

    def spot(i):
        return pl.ds(i * cap, cap)

    def group(g):
        return pl.ds(g * group_rows, group_rows)

    loads = [
        pltpu.make_async_copy(src, dst, load_sem.at[k])
        for k, (src, dst) in enumerate((
            (first_hbm, first_v), (inward_hbm, inward_v), (outward_hbm, outward_v),
            (gate_hbm.at[0], gate_v), (up_hbm.at[0], up_v), (down_hbm.at[0], down_v)))
    ]
    for load in loads:
        load.start()

    barrier = pltpu.get_barrier_semaphore()
    for r in range(1, m):
        pl.semaphore_signal(
            barrier, inc=1, device_id=(2 * lax.rem(a + r, m) + b, t), device_id_type=MESH)
    for step in (1, n - 1):
        pl.semaphore_signal(
            barrier, inc=1, device_id=(lax.rem(me + step, n), t), device_id_type=MESH)
    pl.semaphore_signal(barrier, inc=1, device_id=(me_y, t), device_id_type=MESH)
    for other in (t_core, t_x):
        pl.semaphore_signal(barrier, inc=1, device_id=(me, other), device_id_type=MESH)

    def remote(src, dst, ssem, rsem, ep, tp):
        return pltpu.make_async_remote_copy(
            src_ref=src, dst_ref=dst, send_sem=ssem, recv_sem=rsem,
            device_id=(ep, tp), device_id_type=MESH)

    def side(k, b_side):
        return spot(2 * k + b_side)

    def z_copy(k):
        return remote(sent.at[spot(k)], portion.at[side(k, 0), quarter(t)],
                      zs.at[k], zr.at[k], 2 * lax.rem(a + order[k], m) + b, t)

    def x_copy(k):
        piece = portion.at[side(k, 0), quarter(t)]
        return remote(piece, piece, xs.at[k], xr.at[k], me, t_x)

    def x_arrival(k):
        piece = portion.at[side(k, 0), quarter(t_x)]
        return remote(piece, piece, xs.at[k], xr.at[k], me, t_x)

    def y_copy(k, q):
        cols = quarter((t, t_x)[q])
        return remote(portion.at[side(k, 0), cols], portion.at[side(k, 1), cols],
                      ys.at[k, q], yr.at[k, q], me_y, t)

    def d_copy(k, b_side, q):
        piece = portion.at[side(k, b_side), quarter((t, t_x)[q])]
        return remote(piece, piece, ds.at[k, b_side, q], dr.at[k, b_side, q], me, t_core)

    def d_arrival(k, b_side, q):
        piece = portion.at[side(k, b_side), quarter((t_core, t_diag)[q])]
        return remote(piece, piece, ds.at[k, b_side, q], dr.at[k, b_side, q], me, t_core)

    def r1_copy(g, k):
        return remote(term.at[group(g), quarter((t_core, t_diag)[k])], core_in.at[k, group(g)],
                      r1s.at[g, k], r1r.at[g, k], me, t_core)

    def r2_copy(g):
        return remote(x_out.at[group(g)], x_in.at[group(g)], r2s.at[g], r2r.at[g], me, t_x)

    def r3_copy(k):
        return remote(half_out.at[side(k, 1)], y_in.at[spot(k)], r3s.at[k], r3r.at[k], me_y, t)

    def r4_copy(k):
        return remote(whole_out.at[spot(k)], back.at[spot(k)], r4s.at[k], r4r.at[k],
                      2 * lax.rem(a + m - order[k], m) + b, t)

    def m1_copy(k):
        return remote(mix_term.at[:, quarter((t_core, t_diag)[k])], mix_core.at[k],
                      m1s.at[k], m1r.at[k], me, t_core)

    def m2_copy():
        return remote(mix_x_out, mix_x_in, m2s, m2r, me, t_x)

    def halo_copy():
        return remote(halo_out, halo_in, hs, hr, lax.rem(me + 1, n), t)

    def norm_tile(j, carry):
        tile = pl.ds(pl.multiple_of(j * 64, 64), 64)
        normed[tile, :] = rms(x2[tile, :], gains[:, width:2 * width])
        return carry

    lax.fori_loop(0, rows2 // 64, norm_tile, None)

    before = (lax.broadcasted_iota(jnp.int32, (rows2, rows2), 0)
              < lax.broadcasted_iota(jnp.int32, (rows2, rows2), 1)).astype(BF16)
    places = lax.broadcasted_iota(jnp.int32, (cap, rows2), 0)

    def chosen(k):
        expert = lax.rem(a + order[k], m)
        named = (ids_t[0:1, :] == expert) | (ids_t[1:2, :] == expert)
        flags = jnp.broadcast_to(jnp.where(named, 1.0, 0.0), (16, rows2)).astype(BF16)
        slots = jnp.dot(flags, before, preferred_element_type=F32)[0:1, :].astype(jnp.int32)
        slots = jnp.where(named, slots, -1)
        return jnp.where(places == slots, 1.0, 0.0).astype(BF16)

    pl.semaphore_wait(barrier, m + 4)
    for k in range(1, m):
        sent[spot(k), :] = jnp.dot(
            chosen(k), normed[:, quarter(t)], preferred_element_type=F32).astype(BF16)
        z_copy(k).start()
    own_rows = chosen(0)
    for q in range(parts):
        portion[side(0, 0), q * w:(q + 1) * w] = jnp.dot(
            own_rows, normed[:, q * w:(q + 1) * w], preferred_element_type=F32).astype(BF16)
    y_copy(0, 0).start()
    y_copy(0, 1).start()

    loads[0].wait()
    loads[1].wait()

    def inward_tile(j, carry):
        tile = pl.ds(pl.multiple_of(j * tile1, tile1), tile1)
        later = pl.ds(pl.multiple_of(j * tile1 + 16, 16), tile1)
        rows = rms(first_v[tile, :], gains[:, 0:width])
        product = jnp.dot(rows, inward_v[...], preferred_element_type=F32).astype(BF16)
        extended[later, :] = product.astype(F32)
        return carry

    lax.fori_loop(0, rows1 // tile1, inward_tile, None)
    halo_out[...] = extended[rows1:rows1 + 16, :].astype(BF16)
    halo_copy().start()

    def members(g):
        return range(g * per, (g + 1) * per)

    def arrived(g):
        for k in members(g):
            if k > 0:
                z_copy(k).wait_recv()
                x_copy(k).start()
                y_copy(k, 0).start()
                d_copy(k, 0, 0).start()

    def over_y(g):
        for k in members(g):
            if k > 0:
                x_arrival(k).wait_recv()
                y_copy(k, 1).start()
                d_copy(k, 0, 1).start()

    def to_core(g):
        for k in members(g):
            for q in (0, 1):
                y_copy(k, q).wait_recv()
                d_copy(k, 1, q).start()

    def ready(g):
        for k in members(g):
            for b_side in (0, 1):
                if k > 0 or b_side > 0:
                    for q in (0, 1):
                        d_arrival(k, b_side, q).wait_recv()

    def compute(g):
        unit_tile = min(256, hidden.shape[1])

        def units(j, carry):
            cols = pl.ds(pl.multiple_of(j * unit_tile, unit_tile), unit_tile)
            gate = jnp.dot(portion[group(g), :], gate_v[:, cols], preferred_element_type=F32)
            up = jnp.dot(portion[group(g), :], up_v[:, cols], preferred_element_type=F32)
            hidden[:, cols] = (gate / (1.0 + jnp.exp(-gate)) * up).astype(BF16)
            return carry

        lax.fori_loop(0, hidden.shape[1] // unit_tile, units, None)

        def outs(j, carry):
            cols = quarter(j)
            term[group(g), cols] = jnp.dot(
                hidden[...], down_v[:, cols], preferred_element_type=F32).astype(BF16)
            return carry

        lax.fori_loop(0, parts, outs, None)
        for k in (1, 0):
            r1_copy(g, k).start()

    def over_x(g):
        r1_copy(g, 1).wait_recv()
        x_out[group(g), :] = (term[group(g), quarter(t_x)].astype(F32)
                              + core_in[1, group(g), :].astype(F32)).astype(BF16)
        r2_copy(g).start()

    def home(g):
        r1_copy(g, 0).wait_recv()
        r2_copy(g).wait_recv()
        half_out[group(g), :] = (term[group(g), quarter(t)].astype(F32)
                                 + core_in[0, group(g), :].astype(F32)
                                 + x_in[group(g), :].astype(F32)).astype(BF16)
        for k in members(g):
            r3_copy(k).start()

    def onward(g):
        for k in members(g):
            r3_copy(k).wait_recv()
            whole_out[spot(k), :] = (half_out[side(k, 0), :].astype(F32)
                                     + y_in[spot(k), :].astype(F32)).astype(BF16)
            if k > 0:
                r4_copy(k).start()

    arrived(1)

    halo_copy().wait_recv()
    loads[2].wait()
    extended[0:16, :] = jnp.where(me == 0, 0.0, halo_in[...].astype(F32))
    lanes = min(128, extended.shape[1])
    counts = jnp.minimum(
        me * rows1 + 1 + lax.broadcasted_iota(jnp.int32, (rows1, lanes), 0),
        jnp.left_shift(jnp.int32(2), t)).astype(F32)
    for c in range(extended.shape[1] // lanes):
        cols = slice(c * lanes, (c + 1) * lanes)
        whole = extended[:, cols]
        running, picked = whole, whole
        for level in range(4):
            running = running + pltpu.roll(running, 1 << level, 0)
            picked = jnp.where(t >= level, running, picked)
        mixed[:, cols] = (picked[16:, :] / counts - whole[16:, :]).astype(BF16)
    pooled[...] = (jnp.dot(mixed[...], mixing[0], preferred_element_type=F32)
                   * gains[:, 2 * width:]).astype(BF16)

    def outward_tile(j, carry):
        mix_term[:, quarter(j)] = jnp.dot(
            pooled[...], outward_v[:, quarter(j)], preferred_element_type=F32).astype(BF16)
        return carry

    lax.fori_loop(0, parts, outward_tile, None)
    m1_copy(1).start()
    m1_copy(0).start()

    to_core(0)
    arrived(2)
    over_y(1)
    m1_copy(1).wait_recv()
    mix_x_out[...] = (mix_term[:, quarter(t_x)].astype(F32)
                      + mix_core[1].astype(F32)).astype(BF16)
    m2_copy().start()
    for k in (3, 4, 5):
        loads[k].wait()
    arrived(3)
    ready(0)
    compute(0)
    over_y(2)
    over_y(3)
    to_core(1)
    over_x(0)
    ready(1)
    compute(1)
    to_core(2)
    over_x(1)
    home(0)
    ready(2)
    compute(2)
    to_core(3)
    over_x(2)
    home(1)
    ready(3)
    compute(3)
    over_x(3)
    onward(0)
    onward(1)
    home(2)
    onward(2)

    m1_copy(0).wait_recv()
    m2_copy().wait_recv()
    out1[...] = (mix_term[:, quarter(t)].astype(F32) + mix_core[0].astype(F32)
                 + mix_x_in[...].astype(F32)).astype(BF16)

    after = (lax.broadcasted_iota(jnp.int32, (rows2, rows2), 1)
             < lax.broadcasted_iota(jnp.int32, (rows2, rows2), 0)).astype(BF16)
    tall = lax.broadcasted_iota(jnp.int32, (rows2, cap), 1)
    difference = logits_t[0:1, :] - logits_t[1:2, :]
    lines = lax.broadcasted_iota(jnp.int32, (128, rows2), 0)
    listed = jnp.where(lines == 0, ids_t[0:1, :].astype(F32), ids_t[1:2, :].astype(F32))
    listed = jnp.where(lines == 2, 1.0 / (1.0 + jnp.exp(-difference)), listed)
    listed = jnp.where(lines == 3, 1.0 / (1.0 + jnp.exp(difference)), listed)
    listed = listed.T

    def combine(k, source):
        expert = lax.rem(a + order[k], m).astype(F32)
        is0, is1 = listed[:, 0:1] == expert, listed[:, 1:2] == expert
        named = is0 | is1
        flags = jnp.broadcast_to(jnp.where(named, 1.0, 0.0), (rows2, 128)).astype(BF16)
        slots = jnp.dot(after, flags, preferred_element_type=F32)[:, 0:1].astype(jnp.int32)
        slots = jnp.where(named, slots, -1)
        table = jnp.where(tall == slots, 1.0, 0.0).astype(BF16)
        share = jnp.where(is0, listed[:, 2:3], jnp.where(is1, listed[:, 3:4], 0.0))
        picked = share * jnp.dot(table, source[spot(k), :], preferred_element_type=F32)
        if k == 0:
            total[...] = picked
        else:
            total[...] += picked

    def gather(g):
        for k in members(g):
            if k > 0:
                r4_copy(k).wait_recv()
            combine(k, back if k > 0 else whole_out)

    gather(0)
    home(3)
    gather(1)
    onward(3)
    gather(2)
    gather(3)
    out2[...] = total[...].astype(BF16)

    for k in range(m):
        for q in (0, 1):
            y_copy(k, q).wait_send()
            d_copy(k, 1, q).wait_send()
            if k > 0:
                d_copy(k, 0, q).wait_send()
        r3_copy(k).wait_send()
        if k > 0:
            z_copy(k).wait_send()
            x_copy(k).wait_send()
            r4_copy(k).wait_send()
    for g in range(groups):
        r1_copy(g, 0).wait_send()
        r1_copy(g, 1).wait_send()
        r2_copy(g).wait_send()
    m1_copy(0).wait_send()
    m1_copy(1).wait_send()
    m2_copy().wait_send()
    halo_copy().wait_send()


def local(
    first_input, first_gain, pool_inward, pool_mixing, pool_scale, pool_outward,
    second_input, second_gain, route_ids, route_logits, expert_gate, expert_up, expert_down,
):
    n = lax.axis_size("ep")
    parts = lax.axis_size("tp")
    m = n // 2
    rows1, width = first_input.shape
    rows2 = second_input.shape[0]
    w = width // parts
    cap = 2 * rows2 * 9 // (8 * m)
    cap = -(-cap // 16) * 16
    channels = pool_inward.shape[1]
    units = expert_gate.shape[2]
    slots = n * cap
    gains = lax.optimization_barrier(
        jnp.concatenate([first_gain, second_gain, pool_scale]).astype(F32))[None, :]
    dma = pltpu.SemaphoreType.DMA
    vmem = pl.BlockSpec(memory_space=pltpu.VMEM)
    anywhere = pl.BlockSpec(memory_space=pl.ANY)
    v = pltpu.VMEM
    scratch = [
        v((rows1, width), BF16), v((width, channels), BF16), v((channels, width), BF16),
        v((width, units), BF16), v((width, units), BF16), v((units, width), BF16), dma((6,)),
        v((rows2, width), BF16), v((slots // 2, w), BF16), v((slots, width), BF16),
        v((slots // 4, units), BF16), v((slots, width), BF16), v((2, slots, w), BF16),
        v((slots, w), BF16), v((slots, w), BF16), v((slots, w), BF16), v((slots // 2, w), BF16),
        v((slots // 2, w), BF16), v((slots // 2, w), BF16),
        v((rows2, w), F32),
        v((16, channels), BF16), v((16, channels), BF16), v((rows1 + 16, channels), F32),
        v((rows1, channels), BF16), v((rows1, channels), BF16), v((rows1, width), BF16),
        v((2, rows1, w), BF16), v((rows1, w), BF16), v((rows1, w), BF16),
        dma((m,)), dma((m,)), dma((m,)), dma((m,)),
        dma((m, 2, 2)), dma((m, 2, 2)), dma((m, 2)), dma((m, 2)),
        dma((4, 2)), dma((4, 2)), dma((4,)), dma((4,)), dma((m,)), dma((m,)), dma((m,)), dma((m,)),
        dma(()), dma(()), dma((2,)), dma((2,)), dma(()), dma(()),
    ]
    return pl.pallas_call(
        functools.partial(body, n, parts, cap),
        out_shape=(jax.ShapeDtypeStruct((rows1, w), BF16), jax.ShapeDtypeStruct((rows2, w), BF16)),
        in_specs=[anywhere, vmem, anywhere, vmem, anywhere, vmem, vmem, vmem,
                  anywhere, anywhere, anywhere],
        out_specs=(vmem, vmem),
        scratch_shapes=scratch,
        compiler_params=pltpu.CompilerParams(
            collective_id=0, has_side_effects=True, vmem_limit_bytes=60 * 1024 * 1024),
    )(
        first_input, gains, pool_inward, pool_mixing, pool_outward, second_input,
        route_ids.T, route_logits.T, expert_gate, expert_up, expert_down,
    )


def solution(mesh):
    placed = (
        P("ep", None), P(), P(None, "tp"), P("tp", None, None), P("tp"), P("tp", None),
        P("ep", None), P(), P("ep", None), P("ep", None),
        P("ep", None, "tp"), P("ep", None, "tp"), P("ep", "tp", None),
    )
    return jax.shard_map(
        local, mesh=mesh, in_specs=placed, out_specs=(P("ep", "tp"), P("ep", "tp")), check_vma=False
    )
```

time: 113 us -> 84.2 us (0.75)
  Pallas kernels: 101 us -> 78.3 us
  local copies, waits for them, and re-layouts: 10.3 us -> 4.15 us
    pallas_call x1, Pallas kernels: 101 us -> 78.3 us  [local(): pl.pallas_call(functools.partial(body, n, parts, cap), out_shape=(jax.Sha...]
    broadcast_in_dim x3 -> x1, local copies, waits for them, and re-layouts: 3.81 us -> 0.62 us  [local(): lax.optimization_barrier(jnp.concatenate([first_gain, second_gain, pool_s...]
    unnamed x4 -> x2, local copies, waits for them, and re-layouts: 6.49 us -> 3.54 us
where the time goes in v2:
time: 84.2 us; the launch traced here: 83.8 us
  Pallas kernels  78.3 us (93%)
  local copies, waits for them, and re-layouts  4.15 us (5%)
    pallas_call x1, Pallas kernels, local(): pl.pallas_call(functools.partial(body, n, parts, cap), out_shape=(jax.Sha...  78.3 us
    unnamed x2, local copies, waits for them, and re-layouts  3.54 us

profile of v2, /device:TPU:0, one launch (start us, length us, event | category | flops | bytes accessed | tf_op | source)
XLA Modules:
  0.0 83.8 jit_solution(13196007399064832722)
XLA Ops:
  0.6 0.7 maximum_convert_fusion
  1.4 0.6 broadcast_in_dim.3.gains
  2.0 78.3 %shard_map.140 = (bf16[512,512]{1,0:T(8,128)(2,1)}, bf16[256,512]{1,0:T(8,128)(2,1)}) custom-call(bf16[512,2048]{1,0:T(8,128)(2,1)} %first_hbm.1, f32[1,4352]{1,0:T(1,128)} %broadcast_in_dim.3.gains, bf16[2048,256]{1,0:T(8,128)(2,1)} %inward_hbm.1, bf16[1,256,256]{2,1,0:T(8,128)(2,1)} %mixing.1, bf16[256,2048]{1,0:T(8,128)(2,1)} %outward_hbm.1, ...), custom_call_target="tpu_custom_call" | custom-call | tf_op jit(solution)/shard_map/pallas_call | solution.py:426
  80.3 1.9 %copy.17 = bf16[512,512]{1,0:T(8,128)(2,1)} copy(bf16[512,512]{1,0:T(8,128)(2,1)} %get-tuple-element.4) | data formatting | bytes 1048576
  82.1 1.7 %copy.18 = bf16[256,512]{1,0:T(8,128)(2,1)} copy(bf16[256,512]{1,0:T(8,128)(2,1)} %get-tuple-element.5) | data formatting | bytes 524288

commit v3 on v2

--- a/solution.py
+++ b/solution.py
@@ -116,11 +116,12 @@
         return remote(term.at[group(g), quarter((t_core, t_diag)[k])], core_in.at[k, group(g)],
                       r1s.at[g, k], r1r.at[g, k], me, t_core)
 
-    def r2_copy(g):
-        return remote(x_out.at[group(g)], x_in.at[group(g)], r2s.at[g], r2r.at[g], me, t_x)
+    def r2_copy(k, b_side):
+        rows = side(k, b_side)
+        return remote(x_out.at[rows], x_in.at[rows], r2s.at[k, b_side], r2r.at[k, b_side], me, t_x)
 
     def r3_copy(k):
-        return remote(half_out.at[side(k, 1)], y_in.at[spot(k)], r3s.at[k], r3r.at[k], me_y, t)
+        return remote(half_out.at[spot(k)], y_in.at[spot(k)], r3s.at[k], r3r.at[k], me_y, t)
 
     def r4_copy(k):
         return remote(whole_out.at[spot(k)], back.at[spot(k)], r4s.at[k], r4r.at[k],
@@ -237,24 +238,30 @@
 
     def over_x(g):
         r1_copy(g, 1).wait_recv()
-        x_out[group(g), :] = (term[group(g), quarter(t_x)].astype(F32)
-                              + core_in[1, group(g), :].astype(F32)).astype(BF16)
-        r2_copy(g).start()
+        for b_side in (1, 0):
+            for k in members(g):
+                rows = side(k, b_side)
+                x_out[rows, :] = (term[rows, quarter(t_x)].astype(F32)
+                                  + core_in[1, rows, :].astype(F32)).astype(BF16)
+                r2_copy(k, b_side).start()
+
+    def half_sum(k, b_side):
+        rows = side(k, b_side)
+        return (term[rows, quarter(t)].astype(F32) + core_in[0, rows, :].astype(F32)
+                + x_in[rows, :].astype(F32))
 
     def home(g):
         r1_copy(g, 0).wait_recv()
-        r2_copy(g).wait_recv()
-        half_out[group(g), :] = (term[group(g), quarter(t)].astype(F32)
-                                 + core_in[0, group(g), :].astype(F32)
-                                 + x_in[group(g), :].astype(F32)).astype(BF16)
-        for k in members(g):
+        for k in members(g):
+            r2_copy(k, 1).wait_recv()
+            half_out[spot(k), :] = half_sum(k, 1).astype(BF16)
             r3_copy(k).start()
 
     def onward(g):
         for k in members(g):
+            r2_copy(k, 0).wait_recv()
             r3_copy(k).wait_recv()
-            whole_out[spot(k), :] = (half_out[side(k, 0), :].astype(F32)
-                                     + y_in[spot(k), :].astype(F32)).astype(BF16)
+            whole_out[spot(k), :] = (half_sum(k, 0) + y_in[spot(k), :].astype(F32)).astype(BF16)
             if k > 0:
                 r4_copy(k).start()
 
@@ -319,6 +326,7 @@
     onward(0)
     onward(1)
     home(2)
+    home(3)
     onward(2)
 
     m1_copy(0).wait_recv()
@@ -358,9 +366,8 @@
             combine(k, back if k > 0 else whole_out)
 
     gather(0)
-    home(3)
+    onward(3)
     gather(1)
-    onward(3)
     gather(2)
     gather(3)
     out2[...] = total[...].astype(BF16)
@@ -372,6 +379,8 @@
             if k > 0:
                 d_copy(k, 0, q).wait_send()
         r3_copy(k).wait_send()
+        r2_copy(k, 0).wait_send()
+        r2_copy(k, 1).wait_send()
         if k > 0:
             z_copy(k).wait_send()
             x_copy(k).wait_send()
@@ -379,7 +388,6 @@
     for g in range(groups):
         r1_copy(g, 0).wait_send()
         r1_copy(g, 1).wait_send()
-        r2_copy(g).wait_send()
     m1_copy(0).wait_send()
     m1_copy(1).wait_send()
     m2_copy().wait_send()
@@ -412,7 +420,7 @@
         v((width, units), BF16), v((width, units), BF16), v((units, width), BF16), dma((6,)),
         v((rows2, width), BF16), v((slots // 2, w), BF16), v((slots, width), BF16),
         v((slots // 4, units), BF16), v((slots, width), BF16), v((2, slots, w), BF16),
-        v((slots, w), BF16), v((slots, w), BF16), v((slots, w), BF16), v((slots // 2, w), BF16),
+        v((slots, w), BF16), v((slots, w), BF16), v((slots // 2, w), BF16), v((slots // 2, w), BF16),
         v((slots // 2, w), BF16), v((slots // 2, w), BF16),
         v((rows2, w), F32),
         v((16, channels), BF16), v((16, channels), BF16), v((rows1 + 16, channels), F32),
@@ -420,7 +428,7 @@
         v((2, rows1, w), BF16), v((rows1, w), BF16), v((rows1, w), BF16),
         dma((m,)), dma((m,)), dma((m,)), dma((m,)),
         dma((m, 2, 2)), dma((m, 2, 2)), dma((m, 2)), dma((m, 2)),
-        dma((4, 2)), dma((4, 2)), dma((4,)), dma((4,)), dma((m,)), dma((m,)), dma((m,)), dma((m,)),
+        dma((4, 2)), dma((4, 2)), dma((m, 2)), dma((m, 2)), dma((m,)), dma((m,)), dma((m,)), dma((m,)),
         dma(()), dma(()), dma((2,)), dma((2,)), dma(()), dma(()),
     ]
     return pl.pallas_call(

time: 84.2 us -> 80.1 us (0.951)
  Pallas kernels: 78.3 us -> 74.4 us
    pallas_call x1, Pallas kernels: 78.3 us -> 74.4 us  [local(): pl.pallas_call(functools.partial(body, n, parts, cap), out_shape=(jax.Sha...]
where the time goes in v3:
time: 80.1 us; the launch traced here: 79.9 us
  Pallas kernels  74.4 us (93%)
  local copies, waits for them, and re-layouts  4.15 us (5%)
    pallas_call x1, Pallas kernels, local(): pl.pallas_call(functools.partial(body, n, parts, cap), out_shape=(jax.Sha...  74.4 us
    unnamed x2, local copies, waits for them, and re-layouts  3.54 us

profile of v3, /device:TPU:0, one launch (start us, length us, event | category | flops | bytes accessed | tf_op | source)
XLA Modules:
  0.0 79.9 jit_solution(16570992547487102273)
XLA Ops:
  0.6 0.7 maximum_convert_fusion
  1.4 0.6 broadcast_in_dim.3.gains
  2.0 74.4 %shard_map.140 = (bf16[512,512]{1,0:T(8,128)(2,1)}, bf16[256,512]{1,0:T(8,128)(2,1)}) custom-call(bf16[512,2048]{1,0:T(8,128)(2,1)} %first_hbm.1, f32[1,4352]{1,0:T(1,128)} %broadcast_in_dim.3.gains, bf16[2048,256]{1,0:T(8,128)(2,1)} %inward_hbm.1, bf16[1,256,256]{2,1,0:T(8,128)(2,1)} %mixing.1, bf16[256,2048]{1,0:T(8,128)(2,1)} %outward_hbm.1, ...), custom_call_target="tpu_custom_call" | custom-call | tf_op jit(solution)/shard_map/pallas_call | solution.py:434
  76.3 1.9 %copy.17 = bf16[512,512]{1,0:T(8,128)(2,1)} copy(bf16[512,512]{1,0:T(8,128)(2,1)} %get-tuple-element.4) | data formatting | bytes 1048576
  78.2 1.7 %copy.18 = bf16[256,512]{1,0:T(8,128)(2,1)} copy(bf16[256,512]{1,0:T(8,128)(2,1)} %get-tuple-element.5) | data formatting | bytes 524288
